TPU v7x, 32 devices: a whole 2x2x4 slice. The times are simulated.
32 devices in a mesh: sp: 4 (over z), dp: 8 (over y, x, core).
Axes of the slice: x: 2, y: 2, z: 4, core: 2. Of those that a mesh axis runs over, the one named last changes fastest.
Arguments:
- hidden: bfloat16 [8, 512, 2048], P('dp', 'sp'), may hold values from -6 to 6
- queries: bfloat16 [8, 512, 1024], P('dp', 'sp'), may hold values from -6 to 6
- values: bfloat16 [8, 512, 2048], P('dp', 'sp'), may hold values from -6 to 6
- key_weight: bfloat16 [2048, 1024], P('dp'), may hold values from -0.125 to 0.125
- decay_down: bfloat16 [2048, 16], replicated, may hold values from -0.125 to 0.125
- decay_up: float32 [16, 1024], replicated, may hold values from -1.5 to 1.5
- decay_bias: float32 [1024], replicated, may hold values from -1 to 8
- span_shift: bfloat16 [8, 512], P('dp', 'sp'), may hold values from -1.5 to 1.5, as said below
- norm_gain: float32 [2048], replicated, may hold values from 0.1 to 1.9
Outputs:
- attended: bfloat16 [8, 512, 2048], P('dp', 'sp')
Inputs may be any that keep to these rules, and one draw needn't show every extreme that they name: `span_shift`: constant over each aligned block of 64 positions.
All inputs are finite; a program needn't handle non-finite values.
Results may differ from a plain program's by a relative error of at most 0.0073.
Values may be sent and summed in bfloat16 or wider, within the bound.
A program may use at most 64 MiB of HBM per device.

v0:
```python
import jax
import jax.numpy as jnp
from jax import lax
from jax.sharding import PartitionSpec as P

HEADS = 4
DK = 256
DV = 512
BLOCK = 64
KEY = 1024
VAL = 2048
decay_tau = 16.0
norm_eps = 1e-05
highest = lax.Precision.HIGHEST


def mechanism(query, keys_in, value_in, log_decay):
    length, key_width = query.shape
    value_width = value_in.shape[-1]
    blocks = length // BLOCK
    step_decay = log_decay.reshape(blocks, BLOCK, key_width)
    inclusive = jnp.cumsum(step_decay, axis=1)
    exclusive = inclusive - step_decay
    total = inclusive[:, -1, :]
    query3 = query.reshape(blocks, BLOCK, key_width)
    keys3 = keys_in.reshape(blocks, BLOCK, key_width)
    value_tensor3 = value_in.reshape(blocks, BLOCK, value_width)
    query_forward_part = (query3 * jnp.exp(inclusive)).astype(jnp.bfloat16)
    key_fwd = (keys3 * jnp.exp(-inclusive)).astype(jnp.bfloat16)
    query_reverse_part = (query3 * jnp.exp(-exclusive)).astype(jnp.bfloat16)
    key_bwd = (keys3 * jnp.exp(exclusive)).astype(jnp.bfloat16)
    key_end = (keys3 * jnp.exp(total[:, None, :] - inclusive)).astype(jnp.bfloat16)
    fwd_scores = jnp.einsum(
        "nid,njd->nij", query_forward_part, key_fwd, preferred_element_type=jnp.float32
    )
    bwd_scores = jnp.einsum(
        "nid,njd->nij", query_reverse_part, key_bwd, preferred_element_type=jnp.float32
    )
    row_index = lax.broadcasted_iota(jnp.int32, (BLOCK, BLOCK), 0)
    col_index = lax.broadcasted_iota(jnp.int32, (BLOCK, BLOCK), 1)
    attention_scores = jnp.where((col_index <= row_index)[None], fwd_scores, bwd_scores).astype(
        jnp.bfloat16
    )
    inner_block_term = jnp.einsum(
        "ucy,uyh->uch", attention_scores, value_tensor3, preferred_element_type=jnp.float32
    )
    end_terms = jnp.einsum(
        "njd,nje->nde", key_end, value_tensor3, preferred_element_type=jnp.float32
    )
    start_terms = jnp.einsum(
        "njd,nje->nde", key_bwd, value_tensor3, preferred_element_type=jnp.float32
    )
    rates = jnp.exp(total)

    def forward_step(carry_state, inputs):
        rate, term = inputs
        return (rate[:, None] * carry_state + term, carry_state)

    def backward_step(carry_state, inputs):
        rate, term = inputs
        state_here = rate[:, None] * carry_state
        return (state_here + term, state_here)

    empty = jnp.zeros((key_width, value_width), jnp.float32)
    _, forward_scan_states = lax.scan(forward_step, empty, (rates, end_terms))
    _, reverse_scan_states = lax.scan(backward_step, empty, (rates, start_terms), reverse=True)
    produced_rows = jnp.einsum(
        "tzv,tvg->tzg",
        query_forward_part,
        forward_scan_states.astype(jnp.bfloat16),
        preferred_element_type=jnp.float32,
    )
    produced_rows = produced_rows + jnp.einsum(
        "tzv,tvg->tzg",
        query_reverse_part,
        reverse_scan_states.astype(jnp.bfloat16),
        preferred_element_type=jnp.float32,
    )
    return (inner_block_term + produced_rows).reshape(length, value_width).astype(jnp.bfloat16)


def body(
    hidden, queries, values, key_weight, decay_down, decay_up, decay_bias, span_shift, norm_gain
):
    seq_count, tok_count, model_width = hidden.shape
    group_size = lax.axis_size("sp")
    value_split = group_size // HEADS
    part_width = DV // value_split
    head_index = lax.axis_index("sp") // value_split
    token_rows = hidden.reshape(tok_count, model_width)

    def per_item(tensor, width):
        by_head = tensor.reshape(tok_count, HEADS, width).transpose(1, 0, 2)
        spread_out = jnp.broadcast_to(by_head[:, None], (HEADS, value_split, tok_count, width))
        return spread_out.reshape(group_size, tok_count, width)

    def every_item(tensor):
        return jnp.broadcast_to(tensor[None], (group_size,) + tensor.shape)

    key_sums = jnp.dot(
        token_rows,
        lax.all_gather(key_weight, "dp", axis=0, tiled=True),
        preferred_element_type=jnp.float32,
    )
    keys = key_sums.astype(jnp.bfloat16)
    head_key = lax.all_to_all(per_item(keys, DK), "sp", split_axis=0, concat_axis=1, tiled=True)[0]
    low = jnp.dot(token_rows, decay_down, preferred_element_type=jnp.float32).astype(jnp.bfloat16)
    value_items = values.reshape(tok_count, group_size, part_width).transpose(1, 0, 2)
    head_query, head_value, head_low, head_shift = (
        lax.all_to_all(
            per_item(queries.reshape(tok_count, KEY), DK),
            "sp",
            split_axis=0,
            concat_axis=1,
            tiled=True,
        ),
        lax.all_to_all(value_items, "sp", split_axis=0, concat_axis=1, tiled=True),
        lax.all_to_all(every_item(low), "sp", split_axis=0, concat_axis=1, tiled=True),
        lax.all_to_all(
            every_item(span_shift.reshape(tok_count, 1)),
            "sp",
            split_axis=0,
            concat_axis=1,
            tiled=True,
        ),
    )
    up_columns = lax.dynamic_slice_in_dim(decay_up, head_index * DK, DK, 1)
    bias_part = lax.dynamic_slice_in_dim(decay_bias, head_index * DK, DK, 0)
    pre = jnp.dot(
        head_low[0].astype(jnp.float32),
        up_columns,
        precision=highest,
        preferred_element_type=jnp.float32,
    )
    pre = pre + bias_part[None, :] + head_shift[0].astype(jnp.float32)
    log_decay = jax.nn.log_sigmoid(pre) / decay_tau
    scaled = head_query[0].astype(jnp.float32) * DK ** (-0.5)
    mixed = mechanism(scaled, head_key.astype(jnp.float32), head_value[0], log_decay)
    returned = lax.all_to_all(mixed[None], "sp", split_axis=1, concat_axis=0, tiled=True)
    grouped = returned.astype(jnp.float32).transpose(1, 0, 2).reshape(tok_count, HEADS, DV)
    normed = grouped * lax.rsqrt(jnp.mean(grouped * grouped, axis=-1, keepdims=True) + norm_eps)
    normed = normed * norm_gain.reshape(HEADS, DV)[None]
    return normed.reshape(seq_count, tok_count, VAL).astype(jnp.bfloat16)


def solution(mesh):
    in_specs = (
        P("dp", "sp", None),
        P("dp", "sp", None),
        P("dp", "sp", None),
        P("dp", None),
        P(),
        P(),
        P(),
        P("dp", "sp"),
        P(),
    )
    out_specs = P("dp", "sp", None)
    return jax.shard_map(body, mesh=mesh, in_specs=in_specs, out_specs=out_specs, check_vma=False)
```

profile of v0, /device:TPU:0, one launch (start us, length us, event | category | flops | bytes accessed | tf_op | source)
XLA Modules:
  0.0 159.2 jit_solution(2826352887242074970)
XLA Ops:
  7.3 1.2 broadcast_in_dim.46
  8.5 6.3 %all-to-all-start.2 = ((bf16[4,128,1]{1,2,0:T(2,128)(2,1)}), bf16[4,128,1]{1,2,0:T(2,128)(2,1)S(1)}, u32[]{:S(2)}, u32[]{:S(2)}) async-start(bf16[4,128,1]{1,2,0:T(2,128)(2,1)} %broadcast_in_dim.46), calls=%async_computation.2 | async-start | bytes 4096 | tf_op jit(solution)/shard_map/all_to_all | solution.py:119
  14.8 1.1 convolution_convert_fusion.1
  15.9 4.4 %all-to-all-done.2 = bf16[4,128,1]{1,2,0:T(2,128)(2,1)S(1)} async-done(((bf16[4,128,1]{1,2,0:T(2,128)(2,1)}), bf16[4,128,1]{1,2,0:T(2,128)(2,1)S(1)}, u32[]{:S(2)}, u32[]{:S(2)}) %all-to-all-start.2) | async-done | bytes 1056 | tf_op jit(solution)/shard_map/all_to_all | solution.py:119
  21.0 3.3 %all-to-all-start.1 = ((bf16[4,128,16]{1,2,0:T(8,128)(2,1)}), bf16[4,128,16]{1,2,0:T(8,128)(2,1)S(1)}, u32[]{:S(2)}, u32[]{:S(2)}) async-start(bf16[4,128,16]{1,2,0:T(8,128)(2,1)} %broadcast_in_dim.44), calls=%async_computation.1 | async-start | bytes 32768 | tf_op jit(solution)/shard_map/all_to_all | solution.py:118
  24.2 1.8 %copy.72 = bf16[1,128,1024]{1,2,0:T(8,128)(2,1)} copy(bf16[1,128,1024]{2,1,0:T(8,128)(2,1)} %param.14) | data formatting | bytes 524288 | tf_op args[1]
  26.0 3.8 %all-to-all-done.1 = bf16[4,128,16]{1,2,0:T(8,128)(2,1)S(1)} async-done(((bf16[4,128,16]{1,2,0:T(8,128)(2,1)}), bf16[4,128,16]{1,2,0:T(8,128)(2,1)S(1)}, u32[]{:S(2)}, u32[]{:S(2)}) %all-to-all-start.1) | async-done | bytes 16416 | tf_op jit(solution)/shard_map/all_to_all | solution.py:118
  29.8 3.4 %all-to-all-start = ((bf16[4,128,256]{1,2,0:T(8,128)(2,1)}), bf16[4,128,256]{1,2,0:T(8,128)(2,1)S(1)}, u32[]{:S(2)}, u32[]{:S(2)}) async-start(bf16[4,128,256]{1,2,0:T(8,128)(2,1)} %bitcast.1), calls=%async_computation | async-start | bytes 524288 | tf_op jit(solution)/shard_map/all_to_all | solution.py:110
  33.6 0.9 copy.134
  35.3 13.3 %all-gather.2.cloned.1.call-done = bf16[2048,1024]{1,0:T(8,128)(2,1)} async-done(((bf16[256,1024]{1,0:T(8,128)(2,1)}), bf16[2048,1024]{1,0:T(8,128)(2,1)}) %all-gather.2.cloned.1.call-update) | async-done | bytes 4194320 | tf_op jit(solution)/shard_map/all_gather | solution.py:102
  48.6 2.9 %convolution_convert_fusion = bf16[128,1024]{1,0:T(8,128)(2,1)S(1)} fusion(bf16[2048,1024]{1,0:T(8,128)(2,1)} %all-gather.2.cloned.1.call-done, bf16[1,128,2048]{2,1,0:T(8,128)(2,1)S(1)} %copy-done), kind=kOutput, calls=%fused_computation.18 | convolution fusion | flops 537001984 | bytes 4980736 | tf_op jit(solution)/shard_map/dot_general | solution.py:100
  52.2 4.6 %all-to-all-start.3 = ((bf16[4,128,256]{2,1,0:T(8,128)(2,1)}), bf16[4,128,256]{2,1,0:T(8,128)(2,1)S(1)}, u32[]{:S(2)}, u32[]{:S(2)}) async-start(bf16[4,128,256]{2,1,0:T(8,128)(2,1)} %bitcast.59), calls=%async_computation.3 | async-start | bytes 524288 | tf_op jit(solution)/shard_map/all_to_all | solution.py:106
  56.8 1.4 fusion.12
  59.3 6.8 %all-to-all-done.3 = bf16[4,128,256]{2,1,0:T(8,128)(2,1)S(1)} async-done(((bf16[4,128,256]{2,1,0:T(8,128)(2,1)}), bf16[4,128,256]{2,1,0:T(8,128)(2,1)S(1)}, u32[]{:S(2)}, u32[]{:S(2)}) %all-to-all-start.3) | async-done | bytes 262176 | tf_op jit(solution)/shard_map/all_to_all | solution.py:106
  66.8 3.7 %all-to-all-start.4 = ((bf16[4,128,512]{2,1,0:T(8,128)(2,1)}), bf16[4,128,512]{2,1,0:T(8,128)(2,1)S(1)}, u32[]{:S(2)}, u32[]{:S(2)}) async-start(bf16[4,128,512]{2,1,0:T(8,128)(2,1)} %bitcast.57), calls=%async_computation.4 | async-start | bytes 1048576 | tf_op jit(solution)/shard_map/all_to_all | solution.py:117
  70.6 1.0 copy.73
  71.6 1.0 convert.4
  72.6 3.1 %multiply_convert_fusion.4 = (bf16[8,64,256]{2,0,1:T(8,128)(2,1)}, bf16[8,64,256]{2,0,1:T(8,128)(2,1)S(1)}, bf16[8,64,256]{2,0,1:T(8,128)(2,1)S(1)}, bf16[8,64,256]{2,0,1:T(8,128)(2,1)S(1)}, bf16[8,64,256]{2,0,1:T(8,128)(2,1)}) fusion(f32[8,64,256]{2,0,1:T(8,128)S(1)} %fusion.15, f32[8,64,256]{2,1,0:T(8,128)S(1)} %convert.4, f32[8,64,256]{2,1,0:T(8,128)} %bitcast.82, ...), kind=kLoop, calls=%fused_computation.32 | loop fusion | flops 1835008 | bytes 3416064 | tf_op jit(solution)/shard_map/convert_element_type | solution.py:29
  75.7 7.6 %all-to-all-done.4 = bf16[4,128,512]{2,1,0:T(8,128)(2,1)S(1)} async-done(((bf16[4,128,512]{2,1,0:T(8,128)(2,1)}), bf16[4,128,512]{2,1,0:T(8,128)(2,1)S(1)}, u32[]{:S(2)}, u32[]{:S(2)}) %all-to-all-start.4) | async-done | bytes 524320 | tf_op jit(solution)/shard_map/all_to_all | solution.py:117
  83.3 2.7 %fusion.21 = f32[8,256,512]{2,1,0:T(8,128)} fusion(bf16[8,64,512]{2,1,0:T(8,128)(2,1)S(1)} %bitcast.75, bf16[8,64,256]{2,0,1:T(8,128)(2,1)S(1)} %get-tuple-element.194), kind=kOutput, calls=%fused_computation.43 | convolution fusion | flops 134217728 | bytes 4980736 | tf_op jit(solution)/shard_map/njd,nje->nde/dot_general | solution.py:50
  86.0 1.5 broadcast.22.clone
  87.6 16.1 %while.31 = (s32[]{:T(128)}, f32[256,512]{1,0:T(8,128)S(1)}, bf16[8,256,512]{2,1,0:T(8,128)(2,1)}, f32[8,256]{1,0:T(8,128)S(1)}, f32[8,256,512]{2,1,0:T(8,128)}, /*index=5*/s32[]{:T(128)}, s32[]{:T(128)}, s32[]{:T(128)}) while((s32[]{:T(128)}, f32[256,512]{1,0:T(8,128)S(1)}, bf16[8,256,512]{2,1,0:T(8,128)(2,1)}, ...), condition=%wide.region_4.5_spmd.clone, body=%wide.region_3.4_spmd.clone.sunk | while | flops 655364 | bytes 2625656 | solution.py:66
  88.4 1.2 bitcast_add_fusion.5
  90.4 1.2 bitcast_add_fusion.5
  92.4 1.2 bitcast_add_fusion.5
  93.6 0.8 bitcast_dynamic-update-slice_fusion.5
  94.5 1.2 bitcast_add_fusion.5
  96.5 1.2 bitcast_add_fusion.5
  98.5 1.2 bitcast_add_fusion.5
  100.5 1.2 bitcast_add_fusion.5
  102.5 1.2 bitcast_add_fusion.5
  103.7 2.7 %fusion.17 = f32[8,256,512]{2,1,0:T(8,128)} fusion(bf16[8,64,512]{2,1,0:T(8,128)(2,1)S(1)} %bitcast.76, bf16[8,64,256]{2,0,1:T(8,128)(2,1)S(1)} %copy-done.4), kind=kOutput, calls=%fused_computation.39 | convolution fusion | flops 134217728 | bytes 4980736 | tf_op jit(solution)/shard_map/njd,nje->nde/dot_general | solution.py:47
  106.4 1.5 broadcast.22.clone.1
  107.9 15.5 %while.30 = (s32[]{:T(128)}, f32[256,512]{1,0:T(8,128)S(1)}, bf16[8,256,512]{2,1,0:T(8,128)(2,1)}, f32[8,256]{1,0:T(8,128)S(1)}, f32[8,256,512]{2,1,0:T(8,128)}, /*index=5*/s32[]{:T(128)}, s32[]{:T(128)}) while((s32[]{:T(128)}, f32[256,512]{1,0:T(8,128)S(1)}, bf16[8,256,512]{2,1,0:T(8,128)(2,1)}, f32[8,256]{1,0:T(8,128)S(1)}, ...), condition=%wide.region_2.3_spmd.clone, body=%wide.region_1.2_spmd.clone.sunk | while | flops 524291 | bytes 2362976 | solution.py:65
  108.7 1.2 bitcast_add_fusion.4
  110.6 1.2 bitcast_add_fusion.4
  112.6 1.2 bitcast_add_fusion.4
  114.5 1.2 bitcast_add_fusion.4
  116.4 1.2 bitcast_add_fusion.4
  118.3 1.2 bitcast_add_fusion.4
  120.3 1.2 bitcast_add_fusion.4
  122.2 1.2 bitcast_add_fusion.4
  123.4 2.2 %fusion = f32[8,64,512]{2,1,0:T(8,128)S(1)} fusion(bf16[8,256,512]{2,1,0:T(8,128)(2,1)} %get-tuple-element.136, bf16[8,64,256]{2,0,1:T(8,128)(2,1)S(1)} %get-tuple-element.195), kind=kOutput, calls=%fused_computation.7 | convolution fusion | flops 134217728 | bytes 3407872 | tf_op jit(solution)/shard_map/tzv,tvg->tzg/dot_general | solution.py:73
  128.1 3.8 %reduce = bf16[512,512]{1,0:T(8,128)(2,1)S(1)} reduce(bf16[512,1,512]{2,1,0:T(2,128)(2,1)S(1)} %bitcast.78, bf16[]{:T(256)} %broadcast.39), dimensions={1}, to_apply=%bitcast.60.reduce_sub_computation | reduce | bytes 1048578
  131.9 1.2 reshape.113
  133.1 3.5 %all-to-all-start.5 = ((bf16[4,2,32768]{2,1,0:T(2,128)(2,1)}), bf16[4,2,32768]{2,1,0:T(2,128)(2,1)S(1)}, u32[]{:S(2)}, u32[]{:S(2)}) async-start(bf16[4,2,32768]{2,1,0:T(2,128)(2,1)} %reshape.113), calls=%async_computation.5 | async-start | bytes 1048576 | tf_op jit(solution)/shard_map/all_to_all | solution.py:139
  136.6 13.2 %all-to-all-done.5 = bf16[4,2,32768]{2,1,0:T(2,128)(2,1)S(1)} async-done(((bf16[4,2,32768]{2,1,0:T(2,128)(2,1)}), bf16[4,2,32768]{2,1,0:T(2,128)(2,1)S(1)}, u32[]{:S(2)}, u32[]{:S(2)}) %all-to-all-start.5) | async-done | bytes 524320 | tf_op jit(solution)/shard_map/all_to_all | solution.py:139
  151.2 1.2 convert_element_type.104
  (74 shorter events, 20.7 us)
Async XLA Ops:
  6.5 8.3 %copy-start = (bf16[1,128,2048]{2,1,0:T(8,128)(2,1)S(1)}, bf16[1,128,2048]{2,1,0:T(8,128)(2,1)}, u32[]{:S(2)}) copy-start(bf16[1,128,2048]{2,1,0:T(8,128)(2,1)} %param.13) | copy-start | bytes 1572868
  6.5 26.7 %copy-start.5 = (bf16[1,128,2048]{2,1,0:T(8,128)(2,1)S(1)}, bf16[1,128,2048]{2,1,0:T(8,128)(2,1)}, u32[]{:S(2)}) copy-start(bf16[1,128,2048]{2,1,0:T(8,128)(2,1)} %param.15) | copy-start | bytes 1572868
  6.5 42.0 %all-gather.2.cloned.1.call-start = ((), (), s32[]{:S(2)}) async-start(), calls=%async_computation.6 | async-start | bytes 4718592 | tf_op jit(solution)/shard_map/all_gather | solution.py:102
  8.5 11.8 %all-to-all-start.2 = ((bf16[4,128,1]{1,2,0:T(2,128)(2,1)}), bf16[4,128,1]{1,2,0:T(2,128)(2,1)S(1)}, u32[]{:S(2)}, u32[]{:S(2)}) async-start(bf16[4,128,1]{1,2,0:T(2,128)(2,1)} %broadcast_in_dim.46), calls=%async_computation.2 | async-start | bytes 4096 | tf_op jit(solution)/shard_map/all_to_all | solution.py:119
  21.0 8.8 %all-to-all-start.1 = ((bf16[4,128,16]{1,2,0:T(8,128)(2,1)}), bf16[4,128,16]{1,2,0:T(8,128)(2,1)S(1)}, u32[]{:S(2)}, u32[]{:S(2)}) async-start(bf16[4,128,16]{1,2,0:T(8,128)(2,1)} %broadcast_in_dim.44), calls=%async_computation.1 | async-start | bytes 32768 | tf_op jit(solution)/shard_map/all_to_all | solution.py:118
  29.8 22.4 %all-to-all-start = ((bf16[4,128,256]{1,2,0:T(8,128)(2,1)}), bf16[4,128,256]{1,2,0:T(8,128)(2,1)S(1)}, u32[]{:S(2)}, u32[]{:S(2)}) async-start(bf16[4,128,256]{1,2,0:T(8,128)(2,1)} %bitcast.1), calls=%async_computation | async-start | bytes 524288 | tf_op jit(solution)/shard_map/all_to_all | solution.py:110
  52.2 13.9 %all-to-all-start.3 = ((bf16[4,128,256]{2,1,0:T(8,128)(2,1)}), bf16[4,128,256]{2,1,0:T(8,128)(2,1)S(1)}, u32[]{:S(2)}, u32[]{:S(2)}) async-start(bf16[4,128,256]{2,1,0:T(8,128)(2,1)} %bitcast.59), calls=%async_computation.3 | async-start | bytes 524288 | tf_op jit(solution)/shard_map/all_to_all | solution.py:106
  58.2 0.8 copy-start.2
  66.1 0.7 copy-start.3
  66.8 16.5 %all-to-all-start.4 = ((bf16[4,128,512]{2,1,0:T(8,128)(2,1)}), bf16[4,128,512]{2,1,0:T(8,128)(2,1)S(1)}, u32[]{:S(2)}, u32[]{:S(2)}) async-start(bf16[4,128,512]{2,1,0:T(8,128)(2,1)} %bitcast.57), calls=%async_computation.4 | async-start | bytes 1048576 | tf_op jit(solution)/shard_map/all_to_all | solution.py:117
  87.6 16.1 %copy-start.4 = (bf16[8,64,256]{2,0,1:T(8,128)(2,1)S(1)}, bf16[8,64,256]{2,0,1:T(8,128)(2,1)}, u32[]{:S(2)}) copy-start(bf16[8,64,256]{2,0,1:T(8,128)(2,1)} %get-tuple-element.197) | copy-start | bytes 786436
  123.4 2.2 %copy-start.6 = (bf16[8,64,256]{2,0,1:T(8,128)(2,1)S(1)}, bf16[8,64,256]{2,0,1:T(8,128)(2,1)}, u32[]{:S(2)}) copy-start(bf16[8,64,256]{2,0,1:T(8,128)(2,1)} %get-tuple-element.193) | copy-start | bytes 786436
  123.4 2.4 %copy-start.1 = (bf16[8,256,512]{2,1,0:T(8,128)(2,1)S(1)}, bf16[8,256,512]{2,1,0:T(8,128)(2,1)}, u32[]{:S(2)}) copy-start(bf16[8,256,512]{2,1,0:T(8,128)(2,1)} %get-tuple-element.135) | copy-start | bytes 6291460
  127.5 9.0 %copy-start.7 = (f32[2048]{0:T(1024)S(1)}, f32[2048]{0:T(1024)}, u32[]{:S(2)}) copy-start(f32[2048]{0:T(1024)} %param.21) | copy-start | bytes 24580
  133.1 16.7 %all-to-all-start.5 = ((bf16[4,2,32768]{2,1,0:T(2,128)(2,1)}), bf16[4,2,32768]{2,1,0:T(2,128)(2,1)S(1)}, u32[]{:S(2)}, u32[]{:S(2)}) async-start(bf16[4,2,32768]{2,1,0:T(2,128)(2,1)} %reshape.113), calls=%async_computation.5 | async-start | bytes 1048576 | tf_op jit(solution)/shard_map/all_to_all | solution.py:139
Sparse Core Ops, SparseCore 0:
  9.2 39.2 all-gather.1
where the time goes:
time: 161 us; the launch traced here: 159 us
  waiting for transfers between devices  49.8 us (31%)
  other arithmetic  39.6 us (25%)
  starting transfers between devices  24.7 us (15%)
  local copies, waits for them, and re-layouts  16.8 us (10%)
  matrix products  14.1 us (9%)
  between operations  13.7 us (9%)
    all_gather x1, waiting for transfers between devices, body(): lax.all_gather(key_weight, 'dp', axis=0, tiled=True)  13.3 us
    all_to_all x1, waiting for transfers between devices, body(): lax.all_to_all(mixed[None], 'sp', split_axis=1, concat_axis=0, tiled=True)  13.2 us
    dynamic_update_slice x16, other arithmetic, mechanism(): _, forward_scan_states = lax.scan(forward_step, empty, (rates, end_terms))  12.6 us
    add x8, other arithmetic, forward_step(): return (rate[:, None] * carry_state + term, carry_state)  9.24 us
    add x8, other arithmetic, backward_step(): return (state_here + term, state_here)  9.24 us
    all_to_all x1, waiting for transfers between devices, body(): lax.all_to_all(value_items, 'sp', split_axis=0, concat_axis=1, tiled=True)  7.64 us
    all_to_all x1, waiting for transfers between devices, body(): lax.all_to_all(per_item(keys, DK), 'sp', split_axis=0, concat_axis=1, til...  6.78 us
    all_to_all x1, starting transfers between devices, body(): lax.all_to_all(every_item(span_shift.reshape(tok_count, 1)), 'sp', split_...  6.35 us
  transfers between devices with their start and end apart: 7, of which 6 were waited for; matrix products, arithmetic and copies ran while one was open for 11% of the time, Pallas kernels for 0%

commit v1 on v0

--- a/solution.py
+++ b/solution.py
@@ -136,7 +136,10 @@
     log_decay = jax.nn.log_sigmoid(pre) / decay_tau
     scaled = head_query[0].astype(jnp.float32) * DK ** (-0.5)
     mixed = mechanism(scaled, head_key.astype(jnp.float32), head_value[0], log_decay)
-    returned = lax.all_to_all(mixed[None], "sp", split_axis=1, concat_axis=0, tiled=True)
+    returned = jnp.concatenate(
+        lax.all_to_all(jnp.stack(jnp.split(mixed[None], lax.axis_size("sp"), axis=1)), "sp", 0, 0),
+        axis=0,
+    )
     grouped = returned.astype(jnp.float32).transpose(1, 0, 2).reshape(tok_count, HEADS, DV)
     normed = grouped * lax.rsqrt(jnp.mean(grouped * grouped, axis=-1, keepdims=True) + norm_eps)
     normed = normed * norm_gain.reshape(HEADS, DV)[None]

time: 161 us -> 154 us (0.957)
  local copies, waits for them, and re-layouts: 16.8 us -> 12.2 us
  other arithmetic: 39.6 us -> 36.7 us
    unnamed x3 -> x2, other arithmetic: 3.82 us -> 0.01 us
    unnamed x21 -> x17, local copies, waits for them, and re-layouts: 5.61 us -> 1.85 us
where the time goes in v1:
time: 154 us; the launch traced here: 152 us
  waiting for transfers between devices  50.8 us (33%)
  other arithmetic  36.7 us (24%)
  starting transfers between devices  24.6 us (16%)
  matrix products  14.1 us (9%)
  between operations  13.7 us (9%)
  local copies, waits for them, and re-layouts  12.2 us (8%)
    all_gather x1, waiting for transfers between devices, body(): lax.all_gather(key_weight, 'dp', axis=0, tiled=True)  13.3 us
    all_to_all x1, waiting for transfers between devices, body(): lax.all_to_all(jnp.stack(jnp.split(mixed[None], lax.axis_size('sp'), axis...  13.2 us
    dynamic_update_slice x16, other arithmetic, mechanism(): _, forward_scan_states = lax.scan(forward_step, empty, (rates, end_terms))  12.5 us
    add x8, other arithmetic, backward_step(): return (state_here + term, state_here)  9.24 us
    add x8, other arithmetic, forward_step(): return (rate[:, None] * carry_state + term, carry_state)  9.24 us
    all_to_all x1, waiting for transfers between devices, body(): lax.all_to_all(value_items, 'sp', split_axis=0, concat_axis=1, tiled=True)  7.86 us
    all_to_all x1, waiting for transfers between devices, body(): lax.all_to_all(per_item(keys, DK), 'sp', split_axis=0, concat_axis=1, til...  7.53 us
    all_to_all x1, starting transfers between devices, body(): lax.all_to_all(every_item(span_shift.reshape(tok_count, 1)), 'sp', split_...  6.35 us
  transfers between devices with their start and end apart: 7, of which 6 were waited for; matrix products, arithmetic and copies ran while one was open for 11% of the time, Pallas kernels for 0%

profile of v1, /device:TPU:0, one launch (start us, length us, event | category | flops | bytes accessed | tf_op | source)
XLA Modules:
  0.0 152.4 jit_solution(9707913491749973782)
XLA Ops:
  7.3 1.2 broadcast_in_dim.46
  8.5 6.3 %all-to-all-start.2 = ((bf16[4,128,1]{1,2,0:T(2,128)(2,1)}), bf16[4,128,1]{1,2,0:T(2,128)(2,1)S(1)}, u32[]{:S(2)}, u32[]{:S(2)}) async-start(bf16[4,128,1]{1,2,0:T(2,128)(2,1)} %broadcast_in_dim.46), calls=%async_computation.2 | async-start | bytes 4096 | tf_op jit(solution)/shard_map/all_to_all | solution.py:119
  14.8 1.1 convolution_convert_fusion.1
  15.9 4.4 %all-to-all-done.2 = bf16[4,128,1]{1,2,0:T(2,128)(2,1)S(1)} async-done(((bf16[4,128,1]{1,2,0:T(2,128)(2,1)}), bf16[4,128,1]{1,2,0:T(2,128)(2,1)S(1)}, u32[]{:S(2)}, u32[]{:S(2)}) %all-to-all-start.2) | async-done | bytes 1056 | tf_op jit(solution)/shard_map/all_to_all | solution.py:119
  21.0 3.3 %all-to-all-start.1 = ((bf16[4,128,16]{1,2,0:T(8,128)(2,1)}), bf16[4,128,16]{1,2,0:T(8,128)(2,1)S(1)}, u32[]{:S(2)}, u32[]{:S(2)}) async-start(bf16[4,128,16]{1,2,0:T(8,128)(2,1)} %broadcast_in_dim.44), calls=%async_computation.1 | async-start | bytes 32768 | tf_op jit(solution)/shard_map/all_to_all | solution.py:118
  24.2 1.8 %copy.71 = bf16[1,128,1024]{1,2,0:T(8,128)(2,1)} copy(bf16[1,128,1024]{2,1,0:T(8,128)(2,1)} %param.14) | data formatting | bytes 524288 | tf_op args[1]
  26.0 3.8 %all-to-all-done.1 = bf16[4,128,16]{1,2,0:T(8,128)(2,1)S(1)} async-done(((bf16[4,128,16]{1,2,0:T(8,128)(2,1)}), bf16[4,128,16]{1,2,0:T(8,128)(2,1)S(1)}, u32[]{:S(2)}, u32[]{:S(2)}) %all-to-all-start.1) | async-done | bytes 16416 | tf_op jit(solution)/shard_map/all_to_all | solution.py:118
  29.8 3.4 %all-to-all-start = ((bf16[4,128,256]{1,2,0:T(8,128)(2,1)}), bf16[4,128,256]{1,2,0:T(8,128)(2,1)S(1)}, u32[]{:S(2)}, u32[]{:S(2)}) async-start(bf16[4,128,256]{1,2,0:T(8,128)(2,1)} %bitcast.1), calls=%async_computation | async-start | bytes 524288 | tf_op jit(solution)/shard_map/all_to_all | solution.py:110
  33.6 0.9 copy.130
  35.3 13.3 %all-gather.2.cloned.1.call-done = bf16[2048,1024]{1,0:T(8,128)(2,1)} async-done(((bf16[256,1024]{1,0:T(8,128)(2,1)}), bf16[2048,1024]{1,0:T(8,128)(2,1)}) %all-gather.2.cloned.1.call-update) | async-done | bytes 4194320 | tf_op jit(solution)/shard_map/all_gather | solution.py:102
  48.6 2.9 %convolution_convert_fusion = bf16[128,1024]{1,0:T(8,128)(2,1)S(1)} fusion(bf16[2048,1024]{1,0:T(8,128)(2,1)} %all-gather.2.cloned.1.call-done, bf16[1,128,2048]{2,1,0:T(8,128)(2,1)S(1)} %copy-done), kind=kOutput, calls=%fused_computation.18 | convolution fusion | flops 537001984 | bytes 4980736 | tf_op jit(solution)/shard_map/dot_general | solution.py:100
  52.2 4.6 %all-to-all-start.3 = ((bf16[4,128,256]{2,1,0:T(8,128)(2,1)}), bf16[4,128,256]{2,1,0:T(8,128)(2,1)S(1)}, u32[]{:S(2)}, u32[]{:S(2)}) async-start(bf16[4,128,256]{2,1,0:T(8,128)(2,1)} %bitcast.77), calls=%async_computation.3 | async-start | bytes 524288 | tf_op jit(solution)/shard_map/all_to_all | solution.py:106
  56.8 1.4 fusion.17
  58.6 7.5 %all-to-all-done.3 = bf16[4,128,256]{2,1,0:T(8,128)(2,1)S(1)} async-done(((bf16[4,128,256]{2,1,0:T(8,128)(2,1)}), bf16[4,128,256]{2,1,0:T(8,128)(2,1)S(1)}, u32[]{:S(2)}, u32[]{:S(2)}) %all-to-all-start.3) | async-done | bytes 262176 | tf_op jit(solution)/shard_map/all_to_all | solution.py:106
  66.1 3.5 %all-to-all-start.4 = ((bf16[4,128,512]{2,1,0:T(8,128)(2,1)}), bf16[4,128,512]{2,1,0:T(8,128)(2,1)S(1)}, u32[]{:S(2)}, u32[]{:S(2)}) async-start(bf16[4,128,512]{2,1,0:T(8,128)(2,1)} %bitcast.75), calls=%async_computation.4 | async-start | bytes 1048576 | tf_op jit(solution)/shard_map/all_to_all | solution.py:117
  69.7 1.0 copy.72
  70.7 1.0 convert.4
  71.7 3.1 %multiply_convert_fusion.3 = (bf16[8,64,256]{2,0,1:T(8,128)(2,1)}, bf16[8,64,256]{2,0,1:T(8,128)(2,1)S(1)}, bf16[8,64,256]{2,0,1:T(8,128)(2,1)S(1)}, bf16[8,64,256]{2,0,1:T(8,128)(2,1)S(1)}, bf16[8,64,256]{2,0,1:T(8,128)(2,1)}) fusion(f32[8,64,256]{2,0,1:T(8,128)S(1)} %fusion.20, f32[8,64,256]{2,1,0:T(8,128)S(1)} %convert.4, f32[8,64,256]{2,1,0:T(8,128)} %bitcast.94, ...), kind=kLoop, calls=%fused_computation.37 | loop fusion | flops 1835008 | bytes 3416064 | tf_op jit(solution)/shard_map/convert_element_type | solution.py:29
  74.7 7.9 %all-to-all-done.4 = bf16[4,128,512]{2,1,0:T(8,128)(2,1)S(1)} async-done(((bf16[4,128,512]{2,1,0:T(8,128)(2,1)}), bf16[4,128,512]{2,1,0:T(8,128)(2,1)S(1)}, u32[]{:S(2)}, u32[]{:S(2)}) %all-to-all-start.4) | async-done | bytes 524320 | tf_op jit(solution)/shard_map/all_to_all | solution.py:117
  82.6 2.7 %fusion.26 = f32[8,256,512]{2,1,0:T(8,128)} fusion(bf16[8,64,512]{2,1,0:T(8,128)(2,1)S(1)} %bitcast.90, bf16[8,64,256]{2,0,1:T(8,128)(2,1)S(1)} %get-tuple-element.194), kind=kOutput, calls=%fused_computation.48 | convolution fusion | flops 134217728 | bytes 4980736 | tf_op jit(solution)/shard_map/njd,nje->nde/dot_general | solution.py:50
  85.3 1.5 %broadcast.22.clone = bf16[8,256,512]{2,1,0:T(8,128)(2,1)} broadcast(bf16[]{:T(256)} %constant.115), dimensions={} | broadcast | bytes 2097154 | tf_op jit(solution)/shard_map/broadcast.1
  86.8 16.0 %while.31 = (s32[]{:T(128)}, f32[256,512]{1,0:T(8,128)S(1)}, bf16[8,256,512]{2,1,0:T(8,128)(2,1)}, f32[8,256]{1,0:T(8,128)S(1)}, f32[8,256,512]{2,1,0:T(8,128)}, /*index=5*/s32[]{:T(128)}, s32[]{:T(128)}, s32[]{:T(128)}) while((s32[]{:T(128)}, f32[256,512]{1,0:T(8,128)S(1)}, bf16[8,256,512]{2,1,0:T(8,128)(2,1)}, ...), condition=%wide.region_4.5_spmd.clone, body=%wide.region_3.4_spmd.clone.sunk | while | flops 655364 | bytes 2625656 | solution.py:66
  87.6 1.2 bitcast_add_fusion.5
  89.6 1.2 bitcast_add_fusion.5
  91.6 1.2 bitcast_add_fusion.5
  93.6 1.2 bitcast_add_fusion.5
  95.6 1.2 bitcast_add_fusion.5
  97.7 1.2 bitcast_add_fusion.5
  98.8 0.8 bitcast_dynamic-update-slice_fusion.5
  99.7 1.2 bitcast_add_fusion.5
  100.9 0.8 bitcast_dynamic-update-slice_fusion.5
  101.7 1.2 bitcast_add_fusion.5
  102.9 2.7 %fusion.22 = f32[8,256,512]{2,1,0:T(8,128)} fusion(bf16[8,64,512]{2,1,0:T(8,128)(2,1)S(1)} %bitcast.91, bf16[8,64,256]{2,0,1:T(8,128)(2,1)S(1)} %copy-done.4), kind=kOutput, calls=%fused_computation.44 | convolution fusion | flops 134217728 | bytes 4980736 | tf_op jit(solution)/shard_map/njd,nje->nde/dot_general | solution.py:47
  105.6 1.5 %broadcast.22.clone.1 = bf16[8,256,512]{2,1,0:T(8,128)(2,1)} broadcast(bf16[]{:T(256)} %constant.115), dimensions={} | broadcast | bytes 2097154 | tf_op jit(solution)/shard_map/broadcast.1
  107.1 15.5 %while.30 = (s32[]{:T(128)}, f32[256,512]{1,0:T(8,128)S(1)}, bf16[8,256,512]{2,1,0:T(8,128)(2,1)}, f32[8,256]{1,0:T(8,128)S(1)}, f32[8,256,512]{2,1,0:T(8,128)}, /*index=5*/s32[]{:T(128)}, s32[]{:T(128)}) while((s32[]{:T(128)}, f32[256,512]{1,0:T(8,128)S(1)}, bf16[8,256,512]{2,1,0:T(8,128)(2,1)}, f32[8,256]{1,0:T(8,128)S(1)}, ...), condition=%wide.region_2.3_spmd.clone, body=%wide.region_1.2_spmd.clone.sunk | while | flops 524291 | bytes 2362976 | solution.py:65
  107.9 1.2 bitcast_add_fusion.4
  109.8 1.2 bitcast_add_fusion.4
  111.7 1.2 bitcast_add_fusion.4
  113.7 1.2 bitcast_add_fusion.4
  115.6 1.2 bitcast_add_fusion.4
  117.5 1.2 bitcast_add_fusion.4
  119.5 1.2 bitcast_add_fusion.4
  121.4 1.2 bitcast_add_fusion.4
  122.6 2.2 %fusion = f32[8,64,512]{2,1,0:T(8,128)S(1)} fusion(bf16[8,256,512]{2,1,0:T(8,128)(2,1)} %get-tuple-element.136, bf16[8,64,256]{2,0,1:T(8,128)(2,1)S(1)} %get-tuple-element.195), kind=kOutput, calls=%fused_computation.7 | convolution fusion | flops 134217728 | bytes 3407872 | tf_op jit(solution)/shard_map/tzv,tvg->tzg/dot_general | solution.py:73
  126.0 0.9 pad_maximum_fusion
  126.9 3.5 %all-to-all-start.5 = ((bf16[4,1,128,512]{3,2,1,0:T(8,128)(2,1)}), bf16[4,1,128,512]{3,2,1,0:T(8,128)(2,1)S(1)}, u32[]{:S(2)}, u32[]{:S(2)}) async-start(bf16[4,1,128,512]{3,2,1,0:T(8,128)(2,1)} %pad_maximum_fusion), calls=%async_computation.5 | async-start | bytes 1048576 | tf_op jit(solution)/shard_map/all_to_all | solution.py:140
  130.4 13.2 %all-to-all-done.5 = bf16[4,1,128,512]{3,2,1,0:T(8,128)(2,1)S(1)} async-done(((bf16[4,1,128,512]{3,2,1,0:T(8,128)(2,1)}), bf16[4,1,128,512]{3,2,1,0:T(8,128)(2,1)S(1)}, u32[]{:S(2)}, u32[]{:S(2)}) %all-to-all-start.5) | async-done | bytes 524320 | tf_op jit(solution)/shard_map/all_to_all | solution.py:140
  144.4 1.2 convert_element_type.104
  (70 shorter events, 16.5 us)
Async XLA Ops:
  6.5 8.3 %copy-start = (bf16[1,128,2048]{2,1,0:T(8,128)(2,1)S(1)}, bf16[1,128,2048]{2,1,0:T(8,128)(2,1)}, u32[]{:S(2)}) copy-start(bf16[1,128,2048]{2,1,0:T(8,128)(2,1)} %param.13) | copy-start | bytes 1572868
  6.5 26.7 %copy-start.5 = (bf16[1,128,2048]{2,1,0:T(8,128)(2,1)S(1)}, bf16[1,128,2048]{2,1,0:T(8,128)(2,1)}, u32[]{:S(2)}) copy-start(bf16[1,128,2048]{2,1,0:T(8,128)(2,1)} %param.15) | copy-start | bytes 1572868
  6.5 42.0 %all-gather.2.cloned.1.call-start = ((), (), s32[]{:S(2)}) async-start(), calls=%async_computation.6 | async-start | bytes 4718592 | tf_op jit(solution)/shard_map/all_gather | solution.py:102
  8.5 11.8 %all-to-all-start.2 = ((bf16[4,128,1]{1,2,0:T(2,128)(2,1)}), bf16[4,128,1]{1,2,0:T(2,128)(2,1)S(1)}, u32[]{:S(2)}, u32[]{:S(2)}) async-start(bf16[4,128,1]{1,2,0:T(2,128)(2,1)} %broadcast_in_dim.46), calls=%async_computation.2 | async-start | bytes 4096 | tf_op jit(solution)/shard_map/all_to_all | solution.py:119
  21.0 8.8 %all-to-all-start.1 = ((bf16[4,128,16]{1,2,0:T(8,128)(2,1)}), bf16[4,128,16]{1,2,0:T(8,128)(2,1)S(1)}, u32[]{:S(2)}, u32[]{:S(2)}) async-start(bf16[4,128,16]{1,2,0:T(8,128)(2,1)} %broadcast_in_dim.44), calls=%async_computation.1 | async-start | bytes 32768 | tf_op jit(solution)/shard_map/all_to_all | solution.py:118
  29.8 22.4 %all-to-all-start = ((bf16[4,128,256]{1,2,0:T(8,128)(2,1)}), bf16[4,128,256]{1,2,0:T(8,128)(2,1)S(1)}, u32[]{:S(2)}, u32[]{:S(2)}) async-start(bf16[4,128,256]{1,2,0:T(8,128)(2,1)} %bitcast.1), calls=%async_computation | async-start | bytes 524288 | tf_op jit(solution)/shard_map/all_to_all | solution.py:110
  52.2 13.9 %all-to-all-start.3 = ((bf16[4,128,256]{2,1,0:T(8,128)(2,1)}), bf16[4,128,256]{2,1,0:T(8,128)(2,1)S(1)}, u32[]{:S(2)}, u32[]{:S(2)}) async-start(bf16[4,128,256]{2,1,0:T(8,128)(2,1)} %bitcast.77), calls=%async_computation.3 | async-start | bytes 524288 | tf_op jit(solution)/shard_map/all_to_all | solution.py:106
  58.2 7.9 %copy-start.2 = (f32[512,256]{1,0:T(8,128)}, f32[512,256]{1,0:T(8,128)S(1)}, u32[]{:S(2)}) copy-start(f32[512,256]{1,0:T(8,128)S(1)} %fusion.17) | copy-start | bytes 1572868
  66.1 3.5 %copy-start.3 = (bf16[4,128,256]{2,1,0:T(8,128)(2,1)}, bf16[4,128,256]{2,1,0:T(8,128)(2,1)S(1)}, u32[]{:S(2)}) copy-start(bf16[4,128,256]{2,1,0:T(8,128)(2,1)S(1)} %all-to-all-done.3) | copy-start | bytes 786436
  66.1 16.5 %all-to-all-start.4 = ((bf16[4,128,512]{2,1,0:T(8,128)(2,1)}), bf16[4,128,512]{2,1,0:T(8,128)(2,1)S(1)}, u32[]{:S(2)}, u32[]{:S(2)}) async-start(bf16[4,128,512]{2,1,0:T(8,128)(2,1)} %bitcast.75), calls=%async_computation.4 | async-start | bytes 1048576 | tf_op jit(solution)/shard_map/all_to_all | solution.py:117
  86.8 16.0 %copy-start.4 = (bf16[8,64,256]{2,0,1:T(8,128)(2,1)S(1)}, bf16[8,64,256]{2,0,1:T(8,128)(2,1)}, u32[]{:S(2)}) copy-start(bf16[8,64,256]{2,0,1:T(8,128)(2,1)} %get-tuple-element.197) | copy-start | bytes 786436
  122.6 2.2 %copy-start.6 = (bf16[8,64,256]{2,0,1:T(8,128)(2,1)S(1)}, bf16[8,64,256]{2,0,1:T(8,128)(2,1)}, u32[]{:S(2)}) copy-start(bf16[8,64,256]{2,0,1:T(8,128)(2,1)} %get-tuple-element.193) | copy-start | bytes 786436
  122.6 2.4 %copy-start.1 = (bf16[8,256,512]{2,1,0:T(8,128)(2,1)S(1)}, bf16[8,256,512]{2,1,0:T(8,128)(2,1)}, u32[]{:S(2)}) copy-start(bf16[8,256,512]{2,1,0:T(8,128)(2,1)} %get-tuple-element.135) | copy-start | bytes 6291460
  125.9 4.4 %copy-start.7 = (f32[2048]{0:T(1024)S(1)}, f32[2048]{0:T(1024)}, u32[]{:S(2)}) copy-start(f32[2048]{0:T(1024)} %param.21) | copy-start | bytes 24580
  126.9 16.7 %all-to-all-start.5 = ((bf16[4,1,128,512]{3,2,1,0:T(8,128)(2,1)}), bf16[4,1,128,512]{3,2,1,0:T(8,128)(2,1)S(1)}, u32[]{:S(2)}, u32[]{:S(2)}) async-start(bf16[4,1,128,512]{3,2,1,0:T(8,128)(2,1)} %pad_maximum_fusion), calls=%async_computation.5 | async-start | bytes 1048576 | tf_op jit(solution)/shard_map/all_to_all | solution.py:140
Sparse Core Ops, SparseCore 0:
  9.2 39.2 all-gather.1
